TPU v7x, 32 devices: a whole 2x2x4 slice. The times are simulated.
32 devices in a mesh: kv: 8 (over z, y), tp: 4 (over x, core).
Axes of the slice: x: 2, y: 2, z: 4, core: 2. Of those that a mesh axis runs over, the one named last changes fastest.
Arguments:
- tokens: bfloat16 [16, 4, 4096], P(None, None, 'kv'), may hold values from -20 to 20
- mix_gain: float32 [4096], P('kv'), may hold values from 0.1 to 1.9
- w_query: bfloat16 [4096, 2048], P('kv', 'tp'), may hold values from -0.09375 to 0.09375
- w_key: bfloat16 [4096, 2048], P('kv', 'tp'), may hold values from -0.09375 to 0.09375
- w_value: bfloat16 [4096, 2048], P('kv', 'tp'), may hold values from -0.09375 to 0.09375
- w_forget: bfloat16 [4096, 16], replicated, may hold values from -0.09375 to 0.09375
- forget_bias: float32 [16], P('tp'), may hold values from -1 to 3
- key_cache: bfloat16 [16, 4096, 2048], P(None, 'kv', 'tp'), may hold values from -6 to 6
- value_cache: bfloat16 [16, 4096, 2048], P(None, 'kv', 'tp'), may hold values from -6 to 6
- cum_gate: float32 [16, 16, 4096], P(None, 'tp', 'kv'), may hold values from -761.52 to 0, as said below
- lengths: int32 [16], replicated, may hold values from 1 to 4096, 16381 in all
- w_out: bfloat16 [2048, 4096], P('tp', 'kv'), may hold values from -0.125 to 0.125
- mlp_gain: float32 [4096], P('kv'), may hold values from 0.1 to 1.9
- w_gate: bfloat16 [4096, 11264], P('kv', 'tp'), may hold values from -0.09375 to 0.09375
- w_up: bfloat16 [4096, 11264], P('kv', 'tp'), may hold values from -0.09375 to 0.09375
- w_down: bfloat16 [11264, 4096], P('tp', 'kv'), may hold values from -0.0546875 to 0.0546875
Outputs:
- result: bfloat16 [16, 4, 4096], P(None, None, 'kv')
Inputs may be any that keep to these rules, and one draw needn't show every extreme that they name: `cum_gate`: never rising along positions. `lengths`: one sequence fills all 4096 positions.
All inputs are finite; a program needn't handle non-finite values.
Results may differ from a plain program's by a relative error of at most 0.02.
Values may be sent and summed in bfloat16 or wider, within the bound.
A program may use at most 64 MiB of HBM per device.

v0:
```python
import jax
import jax.numpy as jnp
from jax import lax
from jax.sharding import PartitionSpec as P

D = 4096
EPSILON = 1e-06
NEG_FILL = -1e30


def combined_all(array, axis, combine):
    everything = jax.tree.map(lambda part: lax.all_gather(part, axis), array)
    first = jax.tree.map(lambda part: part[0], everything)

    def turn(k, so_far):
        return combine(so_far, jax.tree.map(lambda part: part[k], everything))

    return lax.fori_loop(1, lax.axis_size(axis), turn, first)


def on_device(
    tokens,
    mix_gain,
    w_query,
    w_key,
    w_value,
    w_forget,
    forget_bias,
    key_cache,
    value_cache,
    cum_gate,
    lengths,
    w_out,
    mlp_gain,
    w_gate,
    w_up,
    w_down,
):
    seq_count, new_count, local_width = tokens.shape
    row_count = seq_count * new_count
    heads_dev = forget_bias.shape[0]
    head_width = w_query.shape[1] // heads_dev
    pos_dev = key_cache.shape[1]
    kv_index = lax.axis_index("kv")
    tp_index = lax.axis_index("tp")
    inputs = tokens.reshape(row_count, local_width).astype(jnp.float32)
    scaled = (inputs * mix_gain).astype(jnp.bfloat16)
    forget_rows = lax.dynamic_slice_in_dim(w_forget, kv_index * local_width, local_width, 0)
    forget_cols = lax.dynamic_slice_in_dim(forget_rows, tp_index * heads_dev, heads_dev, 1)
    query_part = jnp.dot(scaled, w_query, preferred_element_type=jnp.float32)
    key_part = jnp.dot(scaled, w_key, preferred_element_type=jnp.float32)
    value_part = jnp.dot(scaled, w_value, preferred_element_type=jnp.float32)
    forget_part = jnp.dot(scaled, forget_cols, preferred_element_type=jnp.float32)
    squares = jnp.sum(inputs * inputs, axis=1)
    query_sum, key_sum, value_sum, forget_sum, square_sum = (
        lax.psum(query_part.astype(jnp.bfloat16), "kv").astype(jnp.float32),
        lax.psum(key_part.astype(jnp.bfloat16), "kv").astype(jnp.float32),
        lax.psum(value_part.astype(jnp.bfloat16), "kv").astype(jnp.float32),
        lax.psum(forget_part.astype(jnp.bfloat16), "kv").astype(jnp.float32),
        lax.psum(squares.astype(jnp.bfloat16), "kv").astype(jnp.float32),
    )
    inv_norm = lax.rsqrt(square_sum / D + EPSILON)[:, None]
    head_shape = (seq_count, new_count, heads_dev, head_width)
    query = (inv_norm * query_sum).astype(jnp.bfloat16).reshape(head_shape)
    key_new = (inv_norm * key_sum).astype(jnp.bfloat16).reshape(head_shape)
    value_new = (inv_norm * value_sum).astype(jnp.bfloat16).reshape(head_shape)
    log_forget = jax.nn.log_sigmoid(inv_norm * forget_sum + forget_bias).reshape(
        seq_count, new_count, heads_dev
    )
    score_scale = head_width ** (-0.5)
    positions = kv_index * pos_dev + jnp.arange(pos_dev, dtype=jnp.int32)
    live_rows = positions[None, :] < lengths[:, None]
    live_mask = live_rows[:, None, None, :]
    cached_keys = key_cache.reshape(seq_count, pos_dev, heads_dev, head_width)
    cached_values = value_cache.reshape(seq_count, pos_dev, heads_dev, head_width)
    scores = jnp.einsum("bthd,bphd->bthp", query, cached_keys, preferred_element_type=jnp.float32)
    scores = scores * score_scale - cum_gate[:, None]
    scores = jnp.where(live_mask, scores, NEG_FILL)
    block_peak = jnp.max(scores, axis=3)
    weights = jnp.where(live_mask, jnp.exp(scores - block_peak[..., None]), 0.0)
    block_total = jnp.sum(weights, axis=3)
    block_sum = jnp.einsum(
        "bthp,bphd->bthd",
        weights.astype(jnp.bfloat16),
        cached_values,
        preferred_element_type=jnp.float32,
    )
    last_hit = positions[None, :] == (lengths - 1)[:, None]
    last_piece = jnp.sum(jnp.where(last_hit[:, None, :], cum_gate, 0.0), axis=2)

    def combine(first, second):
        peak_both = jnp.maximum(first[0], second[0])
        first_factor = jnp.exp(first[0] - peak_both)
        second_factor = jnp.exp(second[0] - peak_both)
        return (
            peak_both,
            first[1] * first_factor + second[1] * second_factor,
            first[2] * first_factor[..., None] + second[2] * second_factor[..., None],
            first[3] + second[3],
        )

    past_peak, past_total, past_sum, last_cum = combined_all(
        (block_peak, block_total, block_sum, last_piece), "kv", combine
    )
    key_cum = last_cum[:, None, :] + jnp.cumsum(log_forget, axis=1)
    own_scores = (
        jnp.einsum("bthd,bshd->bths", query, key_new, preferred_element_type=jnp.float32)
        * score_scale
    )
    own_scores = own_scores - jnp.transpose(key_cum, (0, 2, 1))[:, None]
    causal = (jnp.arange(new_count)[:, None] >= jnp.arange(new_count)[None, :])[None, :, None, :]
    own_scores = jnp.where(causal, own_scores, NEG_FILL)
    peak_score = jnp.maximum(past_peak, jnp.max(own_scores, axis=3))
    past_factor = jnp.exp(past_peak - peak_score)
    own_weights = jnp.where(causal, jnp.exp(own_scores - peak_score[..., None]), 0.0)
    numerator = past_sum * past_factor[..., None] + jnp.einsum(
        "bths,bshd->bthd",
        own_weights.astype(jnp.bfloat16),
        value_new,
        preferred_element_type=jnp.float32,
    )
    denominator = past_total * past_factor + jnp.sum(own_weights, axis=3)
    attended = (
        (numerator / denominator[..., None])
        .astype(jnp.bfloat16)
        .reshape(row_count, heads_dev * head_width)
    )
    attn_out = lax.psum(
        jnp.dot(attended, w_out, preferred_element_type=jnp.float32).astype(jnp.bfloat16), "tp"
    ).astype(jnp.float32)
    middle = (inputs + attn_out).astype(jnp.bfloat16)
    middle_wide = middle.astype(jnp.float32)
    squares2 = jnp.sum(middle_wide * middle_wide, axis=1)
    scaled2 = (middle_wide * mlp_gain).astype(jnp.bfloat16)
    gate_part = jnp.dot(scaled2, w_gate, preferred_element_type=jnp.float32)
    up_part = jnp.dot(scaled2, w_up, preferred_element_type=jnp.float32)
    gate_sum, up_sum, square_sum2 = (
        lax.psum(gate_part.astype(jnp.bfloat16), "kv").astype(jnp.float32),
        lax.psum(up_part.astype(jnp.bfloat16), "kv").astype(jnp.float32),
        lax.psum(squares2.astype(jnp.bfloat16), "kv").astype(jnp.float32),
    )
    inv_norm2 = lax.rsqrt(square_sum2 / D + EPSILON)[:, None]
    hidden = (jax.nn.silu(inv_norm2 * gate_sum) * (inv_norm2 * up_sum)).astype(jnp.bfloat16)
    down_part = jnp.dot(hidden, w_down, preferred_element_type=jnp.float32)
    mixed = lax.psum(down_part.astype(jnp.bfloat16), "tp").astype(jnp.float32)
    return (middle_wide + mixed).astype(jnp.bfloat16).reshape(seq_count, new_count, local_width)


def solution(mesh):
    in_specs = (
        P(None, None, "kv"),
        P("kv"),
        P("kv", "tp"),
        P("kv", "tp"),
        P("kv", "tp"),
        P(),
        P("tp"),
        P(None, "kv", "tp"),
        P(None, "kv", "tp"),
        P(None, "tp", "kv"),
        P(),
        P("tp", "kv"),
        P("kv"),
        P("kv", "tp"),
        P("kv", "tp"),
        P("tp", "kv"),
    )
    out_specs = P(None, None, "kv")
    return jax.shard_map(
        on_device, mesh=mesh, in_specs=in_specs, out_specs=out_specs, check_vma=False
    )
```

profile of v0, /device:TPU:0, one launch (start us, length us, event | category | flops | bytes accessed | tf_op | source)
XLA Modules:
  0.0 381.2 jit_solution(16673894785011786111)
XLA Ops:
  6.5 1.0 reshape.113
  7.5 0.7 multiply_convert_fusion.5
  8.2 1.9 convolution_convert_fusion.4
  10.1 1.9 convolution_convert_fusion.5
  12.0 1.9 convolution_convert_fusion.6
  13.9 1.0 multiply_reduce_fusion
  14.9 0.7 broadcast_add_fusion
  15.7 1.3 broadcast_compare_fusion
  17.0 0.9 convolution_convert_fusion.7
  17.9 23.7 %all-reduce = (bf16[64]{0:T(256)(128)(2,1)S(1)}, bf16[64,4]{0,1:T(4,128)(2,1)}) all-reduce(bf16[64]{0:T(256)(128)(2,1)S(1)} %convert_element_type.112, bf16[64,4]{0,1:T(4,128)(2,1)S(1)} %convolution_convert_fusion.7), channel_id=1, replica_groups=mesh['kv'=8,'tp'=4] {'kv'}, use_global_device_ids=true, to_apply=%region_1.0 | all-reduce | flops 320 | bytes 1280 | tf_op jit(solution)/shard_map/psum | solution.py:60
  41.7 46.5 %all-reduce.14.cloned.1.call-done = (bf16[64,512]{1,0:T(8,128)(2,1)}, bf16[64,512]{1,0:T(8,128)(2,1)}, bf16[64,512]{1,0:T(8,128)(2,1)}) async-done(((bf16[64,512]{1,0:T(8,128)(2,1)}, bf16[64,512]{1,0:T(8,128)(2,1)}, bf16[64,512]{1,0:T(8,128)(2,1)}), (bf16[64,512]{1,0:T(8,128)(2,1)}, bf16[64,512]{1,0:T(8,128)(2,1)}, bf16[64,512]{1,0:T(8,128)(2,1)})) %all-reduce.14.cloned.1.call-update) | async-done | bytes 196624 | tf_op jit(solution)/shard_map/psum | solution.py:56
  88.1 1.6 multiply_convert_fusion.2
  89.8 0.6 reshape.105
  90.4 5.9 %fusion.55 = (f32[16,4,4]{1,2,0:T(4,128)S(1)}, f32[16,4,4,512]{3,1,2,0:T(4,128)S(1)}) fusion(f32[16,4,512]{2,1,0:T(4,128)} %param.27, bf16[16,4,4,128]{3,2,1,0:T(4,128)(2,1)} %reshape.105, pred[16,512]{1,0:T(8,128)(4,1)S(1)} %get-tuple-element.304, bf16[16,512,512]{2,1,0:T(8,128)(2,1)} %param.25), kind=kOutput, calls=%fused_computation.83 | convolution fusion | flops 34078464 | bytes 9118720 | tf_op jit(solution)/shard_map/bthd,bphd->bthp/dot_general | solution.py:76
  96.3 0.6 copy-done.1
  96.9 1.3 fusion.15
  98.2 0.7 copy.91
  99.0 1.6 select_reduce_fusion
  100.6 0.8 copy.92
  101.4 0.8 fusion.50
  102.2 0.7 reshape.109
  102.9 2.9 reduce_window_sum.11
  105.7 26.1 %all-gather.4 = f32[8,16,4]{1,2,0:T(4,128)S(1)} all-gather(f32[1,16,4]{1,2,0:T(4,128)S(1)} %bitcast.110), channel_id=5, replica_groups=mesh['kv'=8,'tp'=4] {'kv'}, dimensions={0}, use_global_device_ids=true | all-gather | bytes 2304 | tf_op jit(solution)/shard_map/all_gather | solution.py:12
  131.9 0.6 copy-done.2
  132.5 1.5 copy.88
  134.0 1.5 reshape.110
  135.5 1.5 reshape.108
  137.0 1.7 fusion.41
  138.7 1.7 copy.101
  140.4 1.8 fusion.27
  142.2 1.0 copy.89
  143.1 30.9 %all-gather.1 = f32[128,4,4]{2,1,0:T(4,128)S(1)} all-gather(f32[16,4,4]{2,1,0:T(4,128)S(1)} %copy.89), channel_id=3, replica_groups=mesh['kv'=8,'tp'=4] {'kv'}, dimensions={0}, use_global_device_ids=true | all-gather | bytes 9216 | tf_op jit(solution)/shard_map/all_gather | solution.py:12
  174.4 31.0 %all-gather = f32[128,4,4]{2,1,0:T(4,128)S(1)} all-gather(f32[16,4,4]{2,1,0:T(4,128)} %copy.88), channel_id=2, replica_groups=mesh['kv'=8,'tp'=4] {'kv'}, dimensions={0}, use_global_device_ids=true | all-gather | bytes 9216 | tf_op jit(solution)/shard_map/all_gather | solution.py:12
  205.7 0.9 slice.23
  206.7 15.8 %while.21 = (s32[]{:T(128)}, f32[16,4,4]{0,2,1:T(4,128)S(1)}, f32[16,4,4]{0,2,1:T(4,128)S(1)}, f32[16,4,4,128]{3,2,1,0:T(4,128)S(1)}, f32[16,4]{0,1:T(4,128)S(1)...) while((s32[]{:T(128)}, f32[16,4,4]{0,2,1:T(4,128)S(1)}, ...), condition=%wide.region_7.8_spmd, body=%wide.region_6.7_spmd.sunk | while | flops 99909 | bytes 408483 | solution.py:18
  206.7 0.7 bitcast_add_fusion.3
  207.6 1.3 fusion.73
  208.9 0.7 bitcast_add_fusion.3
  209.9 1.3 fusion.73
  211.2 0.7 bitcast_add_fusion.3
  212.1 1.3 fusion.73
  213.5 0.7 bitcast_add_fusion.3
  214.4 1.3 fusion.73
  215.7 0.7 bitcast_add_fusion.3
  216.7 1.3 fusion.73
  218.0 0.7 bitcast_add_fusion.3
  218.9 1.3 fusion.73
  220.2 0.7 bitcast_add_fusion.3
  221.2 1.3 fusion.73
  222.5 0.8 add_bitcast_fusion
  223.4 0.9 fusion.51
  224.3 0.9 fusion.47
  225.4 1.0 fusion.39
  226.6 1.9 convolution_convert_fusion.3
  228.6 29.2 %all-reduce.8.cloned.1.call-done = bf16[64,512]{1,0:T(8,128)(2,1)} async-done(((bf16[64,512]{1,0:T(8,128)(2,1)}), bf16[64,512]{1,0:T(8,128)(2,1)}) %all-reduce.8.cloned.1.call-update) | async-done | bytes 65552 | tf_op jit(solution)/shard_map/psum | solution.py:128
  257.8 1.0 fusion.32
  258.8 2.0 convolution_convert_fusion.1
  260.8 3.2 convolution_convert_fusion
  264.1 21.6 %psum.76 = bf16[64]{0:T(256)(128)(2,1)S(1)} all-reduce(bf16[64]{0:T(256)(128)(2,1)S(1)} %get-tuple-element.297), channel_id=1, replica_groups=mesh['kv'=8,'tp'=4] {'kv'}, use_global_device_ids=true, to_apply=%region_16.17 | all-reduce | flops 64 | bytes 256 | tf_op jit(solution)/shard_map/psum | solution.py:140
  285.7 53.3 %all-reduce.12.cloned.1.call-done = (bf16[64,2816]{1,0:T(8,128)(2,1)}, bf16[64,2816]{1,0:T(8,128)(2,1)}) async-done(((bf16[64,2816]{1,0:T(8,128)(2,1)}, bf16[64,2816]{1,0:T(8,128)(2,1)}), (bf16[64,2816]{1,0:T(8,128)(2,1)}, bf16[64,2816]{1,0:T(8,128)(2,1)})) %all-reduce.12.cloned.1.call-update) | async-done | bytes 720912 | tf_op jit(solution)/shard_map/psum | solution.py:139
  338.9 3.4 convolution_convert_fusion.2
  342.3 30.8 %all-reduce.10.cloned.1.call-done = bf16[64,512]{1,0:T(8,128)(2,1)} async-done(((bf16[64,512]{1,0:T(8,128)(2,1)}), bf16[64,512]{1,0:T(8,128)(2,1)}) %all-reduce.10.cloned.1.call-update) | async-done | bytes 65552 | tf_op jit(solution)/shard_map/psum | solution.py:145
  373.1 0.9 fusion.34
  374.0 0.7 reshape.112
  (58 shorter events, 3.3 us)
Async XLA Ops:
  6.5 252.3 %copy-start = (bf16[512,2816]{1,0:T(8,128)(2,1)S(1)}, bf16[512,2816]{1,0:T(8,128)(2,1)}, u32[]{:S(2)}) copy-start(bf16[512,2816]{1,0:T(8,128)(2,1)} %param.31) | copy-start | bytes 8650756
  6.5 81.6 %all-reduce.14.cloned.1.call-start = ((), (), s32[]{:S(2)}) async-start(), calls=%async_computation.4 | async-start | bytes 393216 | tf_op jit(solution)/shard_map/psum | solution.py:56
  13.9 191.8 %all-gather.7.cloned.1.call-start = ((), (), s32[]{:S(2)}) async-start(), calls=%async_computation.2 | async-start | bytes 1179648 | tf_op jit(solution)/shard_map/all_gather | solution.py:12
  41.7 48.8 %copy-start.3 = (f32[64]{0:T(128)}, f32[64]{0:T(128)S(1)}, u32[]{:S(2)}) copy-start(f32[64]{0:T(128)S(1)} %add_rsqrt_fusion.1) | copy-start | bytes 772
  90.4 6.5 %copy-start.4 = (bf16[16,512,512]{2,1,0:T(8,128)(2,1)S(1)}, bf16[16,512,512]{2,1,0:T(8,128)(2,1)}, u32[]{:S(2)}) copy-start(bf16[16,512,512]{2,1,0:T(8,128)(2,1)} %param.26) | copy-start | bytes 25165828
  96.3 0.6 copy-start.1
  98.9 158.9 %all-reduce.8.cloned.1.call-start = ((), (), s32[]{:S(2)}) async-start(), calls=%async_computation | async-start | bytes 131072 | tf_op jit(solution)/shard_map/psum | solution.py:128
  131.9 0.6 copy-start.2
  228.5 110.4 %all-reduce.12.cloned.1.call-start = ((), (), s32[]{:S(2)}) async-start(), calls=%async_computation.3 | async-start | bytes 1441792 | tf_op jit(solution)/shard_map/psum | solution.py:139
  264.0 109.1 %all-reduce.10.cloned.1.call-start = ((), (), s32[]{:S(2)}) async-start(), calls=%async_computation.1 | async-start | bytes 131072 | tf_op jit(solution)/shard_map/psum | solution.py:145
Sparse Core Ops, SparseCore 0:
  14.0 74.0 all-reduce.13
  99.0 39.8 all-gather.6
  228.7 29.1 all-reduce.7
  264.2 74.7 all-reduce.11
  342.4 30.6 all-reduce.9
where the time goes:
time: 383 us; the launch traced here: 381 us
  waiting for transfers between devices  160 us (42%)
  blocking collectives  133 us (35%)
  other arithmetic  31.2 us (8%)
  matrix products  26.9 us (7%)
  local copies, waits for them, and re-layouts  16.3 us (4%)
  between operations  13.3 us (3%)
    all_gather x3, blocking collectives, combined_all(): everything = jax.tree.map(lambda part: lax.all_gather(part, axis), array)  88 us
    psum x1, waiting for transfers between devices, on_device(): lax.psum(up_part.astype(jnp.bfloat16), 'kv').astype(jnp.float32)  53.3 us
    psum x1, waiting for transfers between devices, on_device(): lax.psum(query_part.astype(jnp.bfloat16), 'kv').astype(jnp.float32)  46.5 us
    psum x1, waiting for transfers between devices, on_device(): mixed = lax.psum(down_part.astype(jnp.bfloat16), 'tp').astype(jnp.float32)  30.8 us
    psum x1, waiting for transfers between devices, on_device(): lax.psum(jnp.dot(attended, w_out, preferred_element_type=jnp.float32).ast...  29.2 us
    psum x1, blocking collectives, on_device(): lax.psum(squares.astype(jnp.bfloat16), 'kv').astype(jnp.float32)  23.7 us
    psum x1, blocking collectives, on_device(): lax.psum(squares2.astype(jnp.bfloat16), 'kv').astype(jnp.float32)  21.6 us
    add x7, other arithmetic, combine(): first[2] * first_factor[..., None] + second[2] * second_factor[..., None]  9.27 us
  transfers between devices with their start and end apart: 5, of which 4 were waited for; matrix products, arithmetic and copies ran while one was open for 6% of the time, Pallas kernels for 0%

commit v1 on v0

--- a/solution.py
+++ b/solution.py
@@ -6,6 +6,11 @@
 D = 4096
 EPSILON = 1e-06
 NEG_FILL = -1e30
+
+
+def summed_here(block, axis):
+    pieces = lax.all_gather(block, axis)
+    return jnp.sum(pieces, axis=0)
 
 
 def combined_all(array, axis, combine):
@@ -53,7 +58,7 @@
     forget_part = jnp.dot(scaled, forget_cols, preferred_element_type=jnp.float32)
     squares = jnp.sum(inputs * inputs, axis=1)
     query_sum, key_sum, value_sum, forget_sum, square_sum = (
-        lax.psum(query_part.astype(jnp.bfloat16), "kv").astype(jnp.float32),
+        summed_here(query_part.astype(jnp.bfloat16), "kv").astype(jnp.float32),
         lax.psum(key_part.astype(jnp.bfloat16), "kv").astype(jnp.float32),
         lax.psum(value_part.astype(jnp.bfloat16), "kv").astype(jnp.float32),
         lax.psum(forget_part.astype(jnp.bfloat16), "kv").astype(jnp.float32),

time: 383 us -> 354 us (0.924)
  waiting for transfers between devices: 160 us -> 113 us
  blocking collectives: 133 us -> 165 us
  other arithmetic: 31.2 us -> 24.1 us
  local copies, waits for them, and re-layouts: 16.3 us -> 12.1 us
    psum x1, waiting for transfers between devices: 46.5 us -> 0.02 us  [on_device(): lax.psum(key_part.astype(jnp.bfloat16), 'kv').astype(jnp.float32)]
    all_gather x0 -> x1, blocking collectives: none -> 31.5 us  [summed_here(): pieces = lax.all_gather(block, axis)]
    add x7, other arithmetic: 4.77 us -> 0.1 us  [combine(): first[3] + second[3]]
  transfers between devices with their start and end apart: 5 -> 5, of which waited for: 4 -> 3; matrix products, arithmetic and copies ran while one was open for 6% -> 8% of each run, Pallas kernels for 0% -> 0%
where the time goes in v1:
time: 354 us; the launch traced here: 352 us
  blocking collectives  165 us (47%)
  waiting for transfers between devices  113 us (32%)
  matrix products  24.4 us (7%)
  other arithmetic  24.1 us (7%)
  between operations  13.3 us (4%)
  local copies, waits for them, and re-layouts  12.1 us (3%)
    all_gather x3, blocking collectives, combined_all(): everything = jax.tree.map(lambda part: lax.all_gather(part, axis), array)  88.3 us
    psum x1, waiting for transfers between devices, on_device(): lax.psum(up_part.astype(jnp.bfloat16), 'kv').astype(jnp.float32)  53.1 us
    all_gather x1, blocking collectives, summed_here(): pieces = lax.all_gather(block, axis)  31.5 us
    psum x1, waiting for transfers between devices, on_device(): mixed = lax.psum(down_part.astype(jnp.bfloat16), 'tp').astype(jnp.float32)  30.8 us
    psum x1, waiting for transfers between devices, on_device(): lax.psum(jnp.dot(attended, w_out, preferred_element_type=jnp.float32).ast...  28.8 us
    psum x1, blocking collectives, on_device(): lax.psum(squares.astype(jnp.bfloat16), 'kv').astype(jnp.float32)  23.8 us
    psum x1, blocking collectives, on_device(): lax.psum(squares2.astype(jnp.bfloat16), 'kv').astype(jnp.float32)  21.6 us
    add x7, other arithmetic, combine(): first[2] * first_factor[..., None] + second[2] * second_factor[..., None]  9.26 us
  transfers between devices with their start and end apart: 5, of which 3 were waited for; matrix products, arithmetic and copies ran while one was open for 8% of the time, Pallas kernels for 0%

profile of v1, /device:TPU:0, one launch (start us, length us, event | category | flops | bytes accessed | tf_op | source)
XLA Modules:
  0.0 352.3 jit_solution(3205862578022344178)
XLA Ops:
  6.5 1.0 reshape.118
  7.5 0.7 multiply_convert_fusion.5
  8.2 1.9 convolution_convert_fusion.4
  10.1 1.9 convolution_convert_fusion.5
  12.1 1.0 multiply_reduce_fusion
  13.0 0.6 iota_add_fusion
  13.6 1.2 broadcast_add_fusion
  14.9 0.9 convolution_convert_fusion.7
  15.8 23.8 %all-reduce = (bf16[64]{0:T(256)(128)(2,1)S(1)}, bf16[64,4]{0,1:T(4,128)(2,1)}) all-reduce(bf16[64]{0:T(256)(128)(2,1)S(1)} %convert_element_type.119, bf16[64,4]{0,1:T(4,128)(2,1)S(1)} %convolution_convert_fusion.7), channel_id=1, replica_groups=mesh['kv'=8,'tp'=4] {'kv'}, use_global_device_ids=true, to_apply=%region_1.0 | all-reduce | flops 320 | bytes 1280 | tf_op jit(solution)/shard_map/psum | solution.py:65
  39.7 0.5 copy-done.4
  40.2 1.2 convolution_convert_fusion.6
  41.5 31.5 %all-gather = bf16[512,512]{1,0:T(8,128)(2,1)S(1)} all-gather(bf16[64,512]{1,0:T(8,128)(2,1)S(1)} %convolution_convert_fusion.6), channel_id=2, replica_groups=mesh['kv'=8,'tp'=4] {'kv'}, dimensions={0}, use_global_device_ids=true | all-gather | bytes 589824 | tf_op jit(solution)/shard_map/all_gather | solution.py:12
  73.0 0.7 reduce_sum.58
  73.7 0.9 reshape.119
  74.6 1.5 broadcast_compare_fusion
  76.1 0.1 multiply_convert_fusion.4
  76.3 6.2 %fusion.55 = (f32[16,4,4]{1,2,0:T(4,128)S(1)}, f32[16,4,4,512]{3,1,2,0:T(4,128)S(1)}) fusion(f32[16,4,512]{2,1,0:T(4,128)} %param.27, bf16[16,4,4,128]{3,2,1,0:T(4,128)(2,1)S(1)} %multiply_convert_fusion.4, pred[16,512]{1,0:T(8,128)(4,1)S(1)} %get-tuple-element.303, bf16[16,512,512]{2,1,0:T(8,128)(2,1)} %param.25), kind=kOutput, calls=%fused_computation.83 | convolution fusion | flops 34078464 | bytes 9118720 | tf_op jit(solution)/shard_map/bthd,bphd->bthp/dot_general | solution.py:81
  82.5 0.6 copy-done.1
  83.1 1.3 fusion.15
  84.4 0.7 copy.89
  85.1 1.6 copy.86
  86.7 1.0 select_reduce_fusion
  87.7 0.6 copy.90
  88.4 0.8 fusion.50
  89.2 0.7 reshape.114
  89.9 1.8 fusion.27
  91.6 1.0 copy.87
  92.6 31.1 %all-gather.2 = f32[128,4,4]{2,1,0:T(4,128)S(1)} all-gather(f32[16,4,4]{2,1,0:T(4,128)S(1)} %copy.87), channel_id=4, replica_groups=mesh['kv'=8,'tp'=4] {'kv'}, dimensions={0}, use_global_device_ids=true | all-gather | bytes 9216 | tf_op jit(solution)/shard_map/all_gather | solution.py:17
  123.8 0.3 copy.96
  124.1 31.0 %all-gather.1 = f32[128,4,4]{2,1,0:T(4,128)S(1)} all-gather(f32[16,4,4]{2,1,0:T(4,128)} %copy.86), channel_id=3, replica_groups=mesh['kv'=8,'tp'=4] {'kv'}, dimensions={0}, use_global_device_ids=true | all-gather | bytes 9216 | tf_op jit(solution)/shard_map/all_gather | solution.py:17
  155.1 0.3 copy.95
  155.4 1.9 reduce_window_sum.11
  157.3 26.2 %all-gather.5 = f32[8,16,4]{1,2,0:T(4,128)S(1)} all-gather(f32[1,16,4]{1,2,0:T(4,128)} %bitcast.112), channel_id=6, replica_groups=mesh['kv'=8,'tp'=4] {'kv'}, dimensions={0}, use_global_device_ids=true | all-gather | bytes 2304 | tf_op jit(solution)/shard_map/all_gather | solution.py:17
  183.5 1.0 multiply_convert_fusion.2
  184.6 1.0 fusion.41
  185.6 0.2 copy.99
  185.8 0.9 slice.23
  186.7 11.3 %while.21 = (s32[]{:T(128)}, f32[16,4,4]{0,2,1:T(4,128)S(1)}, f32[16,4,4]{0,2,1:T(4,128)S(1)}, f32[16,4,4,128]{3,2,1,0:T(4,128)S(1)}, f32[16,4]{0,1:T(4,128)S(1)...) while((s32[]{:T(128)}, f32[16,4,4]{0,2,1:T(4,128)S(1)}, ...), condition=%wide.region_7.8_spmd, body=%wide.region_6.7_spmd.sunk | while | flops 99909 | bytes 408483 | solution.py:23
  186.8 0.1 copy.160
  187.0 1.3 fusion.73
  188.6 1.3 fusion.73
  190.2 1.3 fusion.73
  191.6 0.1 copy.160
  191.8 1.3 fusion.73
  193.4 1.3 fusion.73
  194.8 0.1 copy.160
  195.1 1.3 fusion.73
  196.7 1.3 fusion.73
  198.2 0.1 fusion.51
  198.3 0.1 fusion.47
  198.4 0.2 copy.105
  198.6 0.2 fusion.39
  198.8 0.2 fusion.36
  199.0 1.9 convolution_convert_fusion.3
  201.0 28.8 %all-reduce.8.cloned.1.call-done = bf16[64,512]{1,0:T(8,128)(2,1)} async-done(((bf16[64,512]{1,0:T(8,128)(2,1)}), bf16[64,512]{1,0:T(8,128)(2,1)}) %all-reduce.8.cloned.1.call-update) | async-done | bytes 65552 | tf_op jit(solution)/shard_map/psum | solution.py:133
  229.8 1.0 fusion.32
  230.8 1.4 convolution_convert_fusion.1
  232.1 3.2 convolution_convert_fusion
  235.4 21.6 %psum.68 = bf16[64]{0:T(256)(128)(2,1)S(1)} all-reduce(bf16[64]{0:T(256)(128)(2,1)S(1)} %get-tuple-element.296), channel_id=1, replica_groups=mesh['kv'=8,'tp'=4] {'kv'}, use_global_device_ids=true, to_apply=%region_16.17 | all-reduce | flops 64 | bytes 256 | tf_op jit(solution)/shard_map/psum | solution.py:145
  257.0 53.1 %all-reduce.12.cloned.1.call-done = (bf16[64,2816]{1,0:T(8,128)(2,1)}, bf16[64,2816]{1,0:T(8,128)(2,1)}) async-done(((bf16[64,2816]{1,0:T(8,128)(2,1)}, bf16[64,2816]{1,0:T(8,128)(2,1)}), (bf16[64,2816]{1,0:T(8,128)(2,1)}, bf16[64,2816]{1,0:T(8,128)(2,1)})) %all-reduce.12.cloned.1.call-update) | async-done | bytes 720912 | tf_op jit(solution)/shard_map/psum | solution.py:144
  310.1 3.4 convolution_convert_fusion.2
  313.5 30.8 %all-reduce.10.cloned.1.call-done = bf16[64,512]{1,0:T(8,128)(2,1)} async-done(((bf16[64,512]{1,0:T(8,128)(2,1)}), bf16[64,512]{1,0:T(8,128)(2,1)}) %all-reduce.10.cloned.1.call-update) | async-done | bytes 65552 | tf_op jit(solution)/shard_map/psum | solution.py:150
  344.3 0.9 fusion.34
  345.1 0.7 reshape.117
  (64 shorter events, 2.5 us)
Async XLA Ops:
  6.5 224.2 %copy-start = (bf16[512,2816]{1,0:T(8,128)(2,1)S(1)}, bf16[512,2816]{1,0:T(8,128)(2,1)}, u32[]{:S(2)}) copy-start(bf16[512,2816]{1,0:T(8,128)(2,1)} %param.31) | copy-start | bytes 8650756
  6.5 177.0 %all-reduce.14.cloned.1.call-start = ((), (), s32[]{:S(2)}) async-start(), calls=%async_computation.4 | async-start | bytes 262144 | tf_op jit(solution)/shard_map/psum | solution.py:62
  12.0 173.8 %all-gather.8.cloned.1.call-start = ((), (), s32[]{:S(2)}) async-start(), calls=%async_computation.2 | async-start | bytes 1179648 | tf_op jit(solution)/shard_map/all_gather | solution.py:17
  39.7 0.6 copy-start.4
  74.6 8.5 %copy-start.5 = (bf16[16,512,512]{2,1,0:T(8,128)(2,1)S(1)}, bf16[16,512,512]{2,1,0:T(8,128)(2,1)}, u32[]{:S(2)}) copy-start(bf16[16,512,512]{2,1,0:T(8,128)(2,1)} %param.26) | copy-start | bytes 25165828
  76.3 8.1 %copy-start.2 = (bf16[16,4,4,128]{3,2,1,0:T(4,128)(2,1)}, bf16[16,4,4,128]{3,2,1,0:T(4,128)(2,1)S(1)}, u32[]{:S(2)}) copy-start(bf16[16,4,4,128]{3,2,1,0:T(4,128)(2,1)S(1)} %multiply_convert_fusion.4) | copy-start | bytes 196612
  82.5 0.6 copy-start.1
  85.1 144.7 %all-reduce.8.cloned.1.call-start = ((), (), s32[]{:S(2)}) async-start(), calls=%async_computation | async-start | bytes 131072 | tf_op jit(solution)/shard_map/psum | solution.py:133
  88.4 142.4 %copy-start.3 = (f32[512]{0:T(512)S(1)}, f32[512]{0:T(512)}, u32[]{:S(2)}) copy-start(f32[512]{0:T(512)} %param.30) | copy-start | bytes 6148
  200.9 109.1 %all-reduce.12.cloned.1.call-start = ((), (), s32[]{:S(2)}) async-start(), calls=%async_computation.3 | async-start | bytes 1441792 | tf_op jit(solution)/shard_map/psum | solution.py:144
  235.3 108.9 %all-reduce.10.cloned.1.call-start = ((), (), s32[]{:S(2)}) async-start(), calls=%async_computation.1 | async-start | bytes 131072 | tf_op jit(solution)/shard_map/psum | solution.py:150
Sparse Core Ops, SparseCore 0:
  12.1 73.4 all-reduce.13
  87.7 40.3 all-gather.7
  201.0 28.7 all-reduce.7
  235.5 74.5 all-reduce.11
  313.6 30.6 all-reduce.9
